TPU v7x, 32 devices: a whole 2x2x4 slice. The times are simulated.
32 devices in a mesh: ep: 8 (over z, x), tp: 4 (over y, core).
Axes of the slice: x: 2, y: 2, z: 4, core: 2. Of those that a mesh axis runs over, the one named last changes fastest.
Arguments:
- tokens: bfloat16 [4096, 4096], P('ep', 'tp'), may hold values from -60 to 60
- routes: int32 [4096, 4], P('ep'), may hold values from 0 to 31, all different within a row; in each aligned block of 512 rows (0 to 511, 512 to 1023, ...) at most 128 rows name the same one
- route_weights: float32 [4096, 4], P('ep'), may hold values from 0.1 to 1
- pre_gain: float32 [4096], P('tp'), may hold values from 0.1 to 1.9
- expert_gate: bfloat16 [32, 4096, 512], P('ep', 'tp'), may hold values from -0.09375 to 0.09375
- expert_up: bfloat16 [32, 4096, 512], P('ep', 'tp'), may hold values from -0.09375 to 0.09375
- expert_down: bfloat16 [32, 512, 4096], P('ep', None, 'tp'), may hold values from -1 to 1
- shared_gate: bfloat16 [4096, 512], P('tp'), may hold values from -0.09375 to 0.09375
- shared_up: bfloat16 [4096, 512], P('tp'), may hold values from -0.09375 to 0.09375
- shared_down: bfloat16 [512, 4096], P(None, 'tp'), may hold values from -1 to 1
- post_gain: float32 [4096], P('tp'), may hold values from 0.1 to 1.9
Outputs:
- layer_out: bfloat16 [4096, 4096], P('ep', 'tp')
Inputs may be any that keep to these rules, and one draw needn't show every extreme that they name: `routes`: each row names 4 different experts. Within each aligned block of 512 rows (the tokens of one index of ep) no expert is named more than 128 times, a bound that some block reaches.
All inputs are finite; a program needn't handle non-finite values.
Results may differ from a plain program's by a relative error of at most 0.022.
Values may be sent and summed in bfloat16 or wider, within the bound.
A program may use at most 128 MiB of HBM per device.

v0:
```python
import functools

import jax
import jax.numpy as jnp
from jax import lax
from jax.experimental import pallas as pl
from jax.experimental.pallas import tpu as pltpu
from jax.sharding import PartitionSpec as P

epsilon = 1e-06
MESH = pl.DeviceIdType.MESH
F32, BF16 = jnp.float32, jnp.bfloat16
CHUNKS = 4
TABLE = 16
COLUMNS = 256


def ring_of(groups, width):
    if width < 2 or groups % width or groups // width < 2:
        return list(range(groups))
    depth = groups // width
    cycle = []
    for x in range(width):
        column = range(1, depth) if x % 2 == 0 else range(depth - 1, 0, -1)
        cycle += [z * width + x for z in column]
    return cycle + [x for x in range(width - 1, -1, -1)]


def dot(a, b):
    return jnp.dot(a, b, preferred_element_type=F32)


def dot_nt(a, b):
    return lax.dot_general(a, b, (((1,), (1,)), ((), ())), preferred_element_type=F32)


def iota(shape, axis):
    return lax.broadcasted_iota(jnp.int32, shape, axis).astype(F32)


def layer_kernel(
    cfg,
    tokens_hbm,
    meta_ref,
    gain_ref,
    gate_hbm,
    up_hbm,
    down_hbm,
    sgate_hbm,
    sup_hbm,
    sdown_hbm,
    post_ref,
    out_ref,
    tok,
    xbuf,
    mbuf,
    gate,
    up,
    down,
    sgate,
    sup,
    sdown,
    rows,
    hits,
    parts,
    got1,
    sums,
    got2,
    hid,
    made,
    back,
    farb,
    mix,
    slotv,
    wv,
    rinv,
    rwt,
    earlier,
    eye,
    squares,
    load_sem,
    gs,
    gr,
    ms,
    mr,
    rs,
    rr,
    s1s,
    s1r,
    s2s,
    s2r,
    s3s,
    s3r,
    s4s,
    s4r,
    ns,
    nr,
    credit,
):
    groups, members, experts, cap, fanout, ring, features = cfg
    count, width = out_ref.shape
    reach = groups // 2
    wide = members // 2
    units = gate.shape[2]
    share = units // members
    chunk = count // CHUNKS
    slots = experts * cap
    far = 2 * reach - 1

    group, me = lax.axis_index("ep"), lax.axis_index("tp")
    core, row = lax.rem(me, 2), lax.div(me, 2)
    ahead, behind = jnp.int32(0), jnp.int32(0)
    for i, place in enumerate(ring):
        here = group == place
        ahead = jnp.where(here, ring[(i + 1) % groups], ahead)
        behind = jnp.where(here, ring[(i - 1) % groups], behind)
    gather_to = ({"ep": ahead}, {"ep": behind})
    return_to = ({"ep": behind}, {"ep": ahead})
    partner = {"tp": row * 2 + 1 - core}

    def peer_row(d):
        return lax.rem(row + d, wide)

    def remote(src, dst, send, recv, to):
        return pltpu.make_async_remote_copy(
            src_ref=src, dst_ref=dst, send_sem=send, recv_sem=recv, device_id=to, device_id_type=MESH
        )

    barrier = pltpu.get_barrier_semaphore()
    for to in gather_to:
        pl.semaphore_signal(barrier, inc=1, device_id=to, device_id_type=MESH)
    for d in range(1, members):
        pl.semaphore_signal(
            barrier, inc=1, device_id={"tp": lax.rem(me + d, members)}, device_id_type=MESH
        )

    loads = [
        pltpu.make_async_copy(src, dst, load_sem.at[i])
        for i, (src, dst) in enumerate(
            (
                (tokens_hbm, tok),
                (gate_hbm, gate),
                (up_hbm, up),
                (sgate_hbm, sgate),
                (sup_hbm, sup),
                (down_hbm, down),
                (sdown_hbm, sdown),
            )
        )
    ]
    for load in loads:
        load.start()
    loads[0].wait()

    def piece(c):
        start = c * chunk
        return pl.ds(start if isinstance(c, int) else pl.multiple_of(start, chunk), chunk)

    def gather(d, step, c, first=False, last=False):
        src = 0 if first or isinstance(step, int) and step == 1 else 2 * step - 3 + d
        dst = far if last else 2 * step - 1 + d
        return remote(
            xbuf.at[src, piece(c)],
            xbuf.at[dst, piece(c)],
            gs.at[d, step, c],
            gr.at[d, step, c],
            gather_to[d],
        )

    def gather_meta(d, step, first=False):
        src = 0 if first or isinstance(step, int) and step == 1 else 2 * step - 3 + d
        return remote(
            mbuf.at[src], mbuf.at[2 * step - 1 + d], ms.at[d, step], mr.at[d, step], gather_to[d]
        )

    def half(d):
        return range(CHUNKS // 2) if d == 0 else range(CHUNKS // 2, CHUNKS)

    def scaled(c):
        xbuf[0, piece(c)] = (tok[piece(c)].astype(F32) * gain_ref[...]).astype(BF16)

    for c in range(CHUNKS):
        scaled(c)
    pl.semaphore_wait(barrier, 2 + members - 1)
    for d in range(2):
        gather(d, 1, 0, first=True).start()

    def diagonal(c):
        shape = (chunk, count)
        return iota(shape, 0) + float(c * chunk) == iota(shape, 1)

    def squares_row(which, value_of):
        total = jnp.zeros((1, count), F32)
        for c in range(CHUNKS):
            value = value_of(c)
            column = jnp.sum(value * value, axis=1, keepdims=True)
            total = total + jnp.sum(
                jnp.where(diagonal(c), column, 0.0), axis=0, keepdims=True
            )
        squares[which, me] = jnp.broadcast_to(total, (8, count))

    def exchange_squares(which):
        copies = [
            remote(
                squares.at[which, me],
                squares.at[which, me],
                ns.at[which, d],
                nr.at[which, d],
                {"tp": lax.rem(me + d, members)},
            )
            for d in range(1, members)
        ]
        for copy in copies:
            copy.start()
        for copy in copies:
            copy.wait()
        total = squares[which, 0]
        for q in range(1, members):
            total = total + squares[which, q]
        return lax.rsqrt(total / features + epsilon)

    squares_row(0, lambda c: tok[piece(c)].astype(F32))
    mbuf[0, 0 : 2 * fanout] = meta_ref[...]
    mbuf[0, 2 * fanout :] = exchange_squares(0)
    for d in range(2):
        gather_meta(d, 1, first=True).start()
        for c in range(1, CHUNKS):
            gather(d, 1, c, first=True).start()

    square = (count, count)
    earlier[...] = jnp.where(iota(square, 0) < iota(square, 1), 1.0, 0.0).astype(BF16)
    eye[...] = jnp.where(iota(square, 0) == iota(square, 1), 1.0, 0.0).astype(BF16)

    def poll(step, c):
        for d in range(2):
            if c == 0:
                gather_meta(d, step).wait_recv()

                @pl.when(step + 1 < reach + 1 - d)
                def _():
                    gather_meta(d, step + 1).start()

            gather(d, step, c).wait_recv()

            @pl.when(step + 1 < reach)
            def _():
                gather(d, step + 1, c).start()

            if c in half(d):

                @pl.when(step + 1 == reach)
                def _():
                    gather(d, reach, c, last=True).start()

    def tables(k):
        first = (group * experts).astype(F32)
        wanted = first + iota((TABLE, count), 0)
        present = jnp.zeros((TABLE, count), F32)
        weight = jnp.zeros((TABLE, count), F32)
        for j in range(fanout):
            same = mbuf[k, j : j + 1] == wanted
            present = present + jnp.where(same, 1.0, 0.0)
            weight = weight + jnp.where(same, mbuf[k, fanout + j : fanout + j + 1], 0.0)
        slot = dot(present.astype(BF16), earlier[...])
        slotv[k] = jnp.where(present > 0.0, slot, -1.0)
        wv[k] = weight

    def row_values(at, size, hit, inverse, weight):
        inv = jnp.sum(jnp.where(hit, inverse, 0.0), axis=1, keepdims=True)
        rinv[at : at + size] = jnp.broadcast_to(inv, (size, 128))
        if weight is None:
            rwt[at : at + size] = jnp.ones((size, 128), F32)
        else:
            value = jnp.sum(jnp.where(hit, weight, 0.0), axis=1, keepdims=True)
            rwt[at : at + size] = jnp.broadcast_to(value, (size, 128))

    def put_parts(at, size, g, u):
        for q in range(members):
            parts[q, pl.ds(at, size), 0:share] = g[:, q * share : (q + 1) * share].astype(BF16)
            parts[q, pl.ds(at, size), share : 2 * share] = u[
                :, q * share : (q + 1) * share
            ].astype(BF16)

    def dispatch(blocks, shared):
        n = len(blocks)
        for i, k in enumerate(blocks):
            tables(k)
            inverse = mbuf[k, 2 * fanout : 2 * fanout + 1]
            for e in range(experts):
                hit = iota((cap, count), 0) == slotv[k, e : e + 1]
                hits[e * cap : (e + 1) * cap, 0:count] = jnp.where(hit, 1.0, 0.0).astype(BF16)
                row_values((e * n + i) * cap, cap, hit, inverse, wv[k, e : e + 1])

            def pick(j, carry):
                at = pl.ds(pl.multiple_of(j * COLUMNS, COLUMNS), COLUMNS)
                picked = dot(hits[0:slots, 0:count], xbuf[k, :, at]).astype(BF16)
                for e in range(experts):
                    rows[e, i * cap : (i + 1) * cap, at] = picked[e * cap : (e + 1) * cap]
                return carry

            lax.fori_loop(0, width // COLUMNS, pick, 0)

        def project(e, carry):
            taken = rows[e, 0 : n * cap]
            g, u = dot(taken, gate[e]), dot(taken, up[e])
            put_parts(pl.multiple_of(e * n * cap, n * cap), n * cap, g, u)
            return carry

        lax.fori_loop(0, experts, project, 0)
        if shared:
            inverse = mbuf[0, 2 * fanout : 2 * fanout + 1]
            for c in range(CHUNKS):
                row_values(slots + c * chunk, chunk, diagonal(c), inverse, None)

            def project_shared(c, carry):
                taken = xbuf[0, piece(c)]
                g, u = dot(taken, sgate[...]), dot(taken, sup[...])
                put_parts(pl.multiple_of(slots + c * chunk, 32), chunk, g, u)
                return carry

            lax.fori_loop(0, CHUNKS, project_shared, 0)

    def over_rows(total, body):
        size = 128 if total % 128 == 0 else total

        def run(j, carry):
            body(pl.ds(pl.multiple_of(j * size, size), size))
            return carry

        lax.fori_loop(0, total // size, run, 0)

    def core_copies(slot, total):
        return [
            remote(
                parts.at[y * 2 + 1 - core, pl.ds(0, total)],
                got1.at[slot, y, pl.ds(0, total)],
                s1s.at[slot, y],
                s1r.at[slot, y],
                partner,
            )
            for y in range(wide)
        ]

    def add_core(slot, total):
        def body(at):
            for y in range(wide):
                mine = parts[y * 2 + core, at].astype(F32)
                sums[y, at] = (mine + got1[slot, y, at].astype(F32)).astype(BF16)

        over_rows(total, body)

    def row_copies(total):
        return [
            remote(
                sums.at[peer_row(d), pl.ds(0, total)],
                got2.at[d - 1, pl.ds(0, total)],
                s2s.at[d],
                s2r.at[d],
                {"tp": peer_row(d) * 2 + core},
            )
            for d in range(1, wide)
        ]

    def activate(stage, total):
        def body(at):
            value = sums[row, at].astype(F32)
            for d in range(1, wide):
                value = value + got2[d - 1, at].astype(F32)
            inv = rinv[at, 0:share]
            g, u = value[:, 0:share] * inv, value[:, share : 2 * share] * inv
            hidden = g / (1.0 + jnp.exp(-g)) * u * rwt[at, 0:share]
            hid[stage, me, at] = hidden.astype(BF16)

        over_rows(total, body)

    def hidden_row_copies(stage, total):
        return [
            remote(
                hid.at[stage, me, pl.ds(0, total)],
                hid.at[stage, me, pl.ds(0, total)],
                s3s.at[d],
                s3r.at[d],
                {"tp": peer_row(d) * 2 + core},
            )
            for d in range(1, wide)
        ]

    def hidden_core_copies(stage, total):
        return [
            remote(
                hid.at[stage, y * 2 + core, pl.ds(0, total)],
                hid.at[stage, y * 2 + core, pl.ds(0, total)],
                s4s.at[lax.rem(stage, 2), y],
                s4r.at[lax.rem(stage, 2), y],
                partner,
            )
            for y in range(wide)
        ]

    def start(copies):
        for copy in copies:
            copy.start()

    def wait(copies):
        for copy in copies:
            copy.wait()

    def combine(stage, blocks, put):
        n = len(blocks)

        def produce(e, carry):
            at = pl.ds(pl.multiple_of(e * n * cap, n * cap), n * cap)
            taken = jnp.concatenate([hid[stage, q, at] for q in range(members)], axis=1)
            result = dot(taken, down[e]).astype(BF16)
            for i in range(n):
                made[i, pl.ds(pl.multiple_of(e * cap, cap), cap)] = result[i * cap : (i + 1) * cap]
            return carry

        lax.fori_loop(0, experts, produce, 0)
        for i, k in enumerate(blocks):
            slot_column = dot_nt(eye[...], slotv[k].astype(BF16))
            for e in range(experts):
                hit = iota((count, cap), 1) == slot_column[:, e : e + 1]
                hits[0:count, e * cap : (e + 1) * cap] = jnp.where(hit, 1.0, 0.0).astype(BF16)

            def tile(j, carry):
                at = pl.ds(pl.multiple_of(j * COLUMNS, COLUMNS), COLUMNS)
                put(i, at, dot(hits[0:count, 0:slots], made[i, :, at]))
                return carry

            lax.fori_loop(0, width // COLUMNS, tile, 0)

    first_rows = slots + count
    pair_rows = 2 * slots

    for i in range(1, 5):
        loads[i].wait()
    dispatch([0], True)
    start(core_copies(0, first_rows))
    poll(1, 0)
    wait(core_copies(0, first_rows))
    add_core(0, first_rows)
    start(row_copies(first_rows))
    poll(1, 1)
    poll(1, 2)
    wait(row_copies(first_rows))
    activate(0, first_rows)
    start(hidden_row_copies(0, first_rows))
    poll(1, 3)

    def before(s, total_before):
        wait(hidden_row_copies(s - 1, total_before))
        start(hidden_core_copies(s - 1, total_before))

    def run_stage(s, carry):
        @pl.when(s == 2)
        def _():
            wait(hidden_core_copies(0, first_rows))

        @pl.when(s > 2)
        def _():
            wait(hidden_core_copies(s - 2, pair_rows))

        dispatch([2 * s - 1, 2 * s], False)
        slot = lax.rem(s, 2)
        start(core_copies(slot, pair_rows))

        def more(c):
            @pl.when(s + 1 < reach)
            def _():
                poll(s + 1, c)

        more(0)
        wait(core_copies(slot, pair_rows))
        add_core(slot, pair_rows)

        @pl.when(s == 1)
        def _():
            before(1, first_rows)

        @pl.when(s > 1)
        def _():
            before(s, pair_rows)

        start(row_copies(pair_rows))
        more(1)
        more(2)
        wait(row_copies(pair_rows))
        activate(s, pair_rows)
        start(hidden_row_copies(s, pair_rows))
        more(3)
        return carry

    lax.fori_loop(1, reach, run_stage, 0)

    wait(hidden_core_copies(reach - 2, pair_rows if reach > 2 else first_rows))
    gather_meta(0, reach).wait_recv()
    for d in range(2):
        for c in half(d):
            gather(d, reach, c, last=True).wait_recv()
    dispatch([far], False)
    start(core_copies(reach % 2, slots))

    def sent(step, carry):
        for d in range(2):
            for c in range(CHUNKS):
                gather(d, step, c).wait_send()
            gather_meta(d, step).wait_send()
        return carry

    for d in range(2):
        for c in range(CHUNKS):
            gather(d, 1, c, first=True).wait_send()
        gather_meta(d, 1, first=True).wait_send()
        for c in half(d):
            gather(d, reach, c, last=True).wait_send()
    lax.fori_loop(2, reach, sent, 0)
    gather_meta(0, reach).wait_send()
    pl.semaphore_signal(credit.at[1], inc=1, device_id=return_to[0], device_id_type=MESH)
    pl.semaphore_signal(credit.at[0], inc=1, device_id=return_to[1], device_id_type=MESH)

    wait(core_copies(reach % 2, slots))
    add_core(reach % 2, slots)
    before(reach, pair_rows)
    start(row_copies(slots))
    wait(hidden_core_copies(reach - 1, pair_rows))

    def give(d, step, c, source):
        return remote(
            source.at[piece(c)],
            xbuf.at[2 * step - 1 + d, piece(c)],
            rs.at[d, step, c],
            rr.at[d, step, c],
            return_to[d],
        )

    def ready(s):
        def put(i, at, value):
            back[s % 2 if isinstance(s, int) else lax.rem(s, 2), i, :, at] = value.astype(BF16)

        combine(s, [2 * s - 1, 2 * s], put)

    loads[5].wait()
    ready(reach - 1)
    top = back.at[(reach - 1) % 2]
    for d in range(2):
        pl.semaphore_wait(credit.at[d], 1)
    order = [list(half(1)) + list(half(0)), list(half(0)) + list(half(1))]
    for j in range(CHUNKS // 2):
        for d in range(2):
            c = order[d][j]
            give(d, 2, c, top.at[d]).start()

    wait(row_copies(slots))
    activate(reach, slots)
    start(hidden_row_copies(reach, slots))
    wait(hidden_row_copies(reach, slots))
    start(hidden_core_copies(reach, slots))
    wait(hidden_core_copies(reach, slots))

    def put_far(i, at, value):
        farb[:, at] = value.astype(BF16)

    combine(reach, [far], put_far)
    for j in range(CHUNKS // 2):
        for d in range(2):
            c = order[d][CHUNKS // 2 + j]
            give(d, 1, c, farb).start()
    if reach > 2:
        ready(reach - 2)

    def merge(d, step, c, source):
        give(d, step - 1, c, source).wait_recv()
        own = source[piece(c)].astype(F32)
        source[piece(c)] = (own + xbuf[2 * step - 3 + d, piece(c)].astype(F32)).astype(BF16)
        give(d, step, c, source).start()

    for j in range(CHUNKS // 2):
        for d in range(2):
            merge(d, 2, order[d][CHUNKS // 2 + j], top.at[d])

    for d in range(2):
        for c in half(d):
            give(d, 1, c, farb).wait_send()

    def returning(step, carry):
        s = reach + 1 - step
        now = back.at[lax.rem(s, 2)]
        for j in range(CHUNKS):
            for d in range(2):
                merge(d, step, order[d][j], now.at[d])
        for d in range(2):
            for c in range(CHUNKS):
                give(d, step - 1, c, back.at[lax.rem(s + 1, 2), d]).wait_send()

        @pl.when(s > 1)
        def _():
            ready(s - 1)

        return carry

    lax.fori_loop(3, reach + 1, returning, 0)

    loads[6].wait()

    def put_own(i, at, value):
        taken = jnp.concatenate(
            [hid[0, q, slots : slots + count] for q in range(members)], axis=1
        )
        mix[:, at] = value + dot(taken, sdown[:, at])

    combine(0, [0], put_own)
    for d in range(2):
        for c in range(CHUNKS):
            give(d, reach, c, back.at[1, d]).wait_send()
    for j in range(CHUNKS):
        for d in range(2):
            c = order[d][j]
            give(d, reach, c, back.at[1, d]).wait_recv()
            mix[piece(c)] = mix[piece(c)] + xbuf[2 * reach - 1 + d, piece(c)].astype(F32)
    squares_row(1, lambda c: mix[piece(c)])
    scale = exchange_squares(1)[0:1]
    for c in range(CHUNKS):
        column = jnp.sum(jnp.where(diagonal(c), scale, 0.0), axis=1, keepdims=True)
        out_ref[piece(c)] = (mix[piece(c)] * column * post_ref[...]).astype(BF16)


def per_device(
    tokens,
    routes,
    route_weights,
    pre_gain,
    expert_gate,
    expert_up,
    expert_down,
    shared_gate,
    shared_up,
    shared_down,
    post_gain,
):
    members, groups = lax.axis_size("tp"), lax.axis_size("ep")
    count, width = tokens.shape
    fanout = routes.shape[1]
    experts, _, units = expert_gate.shape
    cap = 2 * count * fanout // (experts * groups)
    ring = tuple(ring_of(groups, members // 2))
    reach, wide = groups // 2, members // 2
    slots = experts * cap
    most = max(2 * slots, slots + count)
    share = units // members
    meta = jnp.concatenate([routes.astype(F32), route_weights], axis=1).T
    cfg = (groups, members, experts, cap, fanout, ring, float(width * members))

    vmem = pl.BlockSpec(memory_space=pltpu.VMEM)
    anywhere = pl.BlockSpec(memory_space=pl.ANY)
    dma = pltpu.SemaphoreType.DMA
    steps = reach + 1
    return pl.pallas_call(
        functools.partial(layer_kernel, cfg),
        out_shape=jax.ShapeDtypeStruct((count, width), BF16),
        in_specs=[anywhere, vmem, vmem] + [anywhere] * 6 + [vmem],
        out_specs=vmem,
        scratch_shapes=[
            pltpu.VMEM((count, width), BF16),
            pltpu.VMEM((groups + 1, count, width), BF16),
            pltpu.VMEM((groups, 2 * fanout + 8, count), F32),
            pltpu.VMEM(expert_gate.shape, BF16),
            pltpu.VMEM(expert_up.shape, BF16),
            pltpu.VMEM(expert_down.shape, BF16),
            pltpu.VMEM(shared_gate.shape, BF16),
            pltpu.VMEM(shared_up.shape, BF16),
            pltpu.VMEM(shared_down.shape, BF16),
            pltpu.VMEM((experts, 2 * cap, width), BF16),
            pltpu.VMEM((max(slots, count), max(slots, count)), BF16),
            pltpu.VMEM((members, most, 2 * share), BF16),
            pltpu.VMEM((2, wide, most, 2 * share), BF16),
            pltpu.VMEM((wide, most, 2 * share), BF16),
            pltpu.VMEM((wide - 1, most, 2 * share), BF16),
            pltpu.VMEM((reach + 1, members, most, share), BF16),
            pltpu.VMEM((2, slots, width), BF16),
            pltpu.VMEM((2, 2, count, width), BF16),
            pltpu.VMEM((count, width), BF16),
            pltpu.VMEM((count, width), F32),
            pltpu.VMEM((groups, TABLE, count), F32),
            pltpu.VMEM((groups, TABLE, count), F32),
            pltpu.VMEM((most, 128), F32),
            pltpu.VMEM((most, 128), F32),
            pltpu.VMEM((count, count), BF16),
            pltpu.VMEM((count, count), BF16),
            pltpu.VMEM((2, members, 8, count), F32),
            dma((7,)),
            dma((2, steps, CHUNKS)),
            dma((2, steps, CHUNKS)),
            dma((2, steps)),
            dma((2, steps)),
            dma((2, steps, CHUNKS)),
            dma((2, steps, CHUNKS)),
            dma((2, wide)),
            dma((2, wide)),
            dma((wide,)),
            dma((wide,)),
            dma((wide,)),
            dma((wide,)),
            dma((2, wide)),
            dma((2, wide)),
            dma((2, members)),
            dma((2, members)),
            pltpu.SemaphoreType.REGULAR((2,)),
        ],
        compiler_params=pltpu.CompilerParams(
            collective_id=0, has_side_effects=True, vmem_limit_bytes=67043328
        ),
        name="layer",
    )(
        tokens,
        meta,
        pre_gain[None, :],
        expert_gate,
        expert_up,
        expert_down,
        shared_gate,
        shared_up,
        shared_down,
        post_gain[None, :],
    )


def solution(mesh):
    in_specs = (
        P("ep", "tp"),
        P("ep", None),
        P("ep", None),
        P("tp"),
        P("ep", "tp", None),
        P("ep", "tp", None),
        P("ep", None, "tp"),
        P("tp", None),
        P("tp", None),
        P(None, "tp"),
        P("tp"),
    )
    return jax.shard_map(
        per_device, mesh=mesh, in_specs=in_specs, out_specs=P("ep", "tp"), check_vma=False
    )
```

profile of v0, /device:TPU:0, one launch (start us, length us, event | category | flops | bytes accessed | tf_op | source)
XLA Modules:
  0.0 205.9 jit_solution(1734901813039652663)
XLA Ops:
  0.0 0.7 convert_element_type.3
  0.7 1.3 maximum_bitcast_fusion.meta_ref
  2.0 201.6 %layer.1 = bf16[512,1024]{1,0:T(8,128)(2,1)} custom-call(bf16[512,1024]{1,0:T(8,128)(2,1)} %tokens_hbm.1, f32[8,512]{1,0:T(8,128)} %maximum_bitcast_fusion.meta_ref, f32[1,1024]{1,0:T(1,128)} %bitcast.4, bf16[4,1024,512]{2,1,0:T(8,128)(2,1)} %gate_hbm.1, bf16[4,1024,512]{2,1,0:T(8,128)(2,1)} %up_hbm.1, bf16[4,512,1024]{2,1,0:T(8,128)(2,1)} %down_hbm.1, ...), custom_call_target="tpu_custom_call" | custom-call | tf_op jit(solution)/shard_map/layer/pallas_call | solution.py:658
  203.6 2.3 %copy.13 = bf16[512,1024]{1,0:T(8,128)(2,1)} copy(bf16[512,1024]{1,0:T(8,128)(2,1)} %layer.1) | data formatting | bytes 2097152
where the time goes:
time: 206 us
  Pallas kernels  202 us (98%)
  local copies, waits for them, and re-layouts  2.26 us (1%)
    pallas_call x1, Pallas kernels, per_device(): pl.pallas_call(functools.partial(layer_kernel, cfg), out_shape=jax.ShapeD...  202 us

commit v1 on v0

v1 whole, which is shorter than its diff:
```python
import functools

import jax
import jax.numpy as jnp
from jax import lax
from jax.experimental import pallas as pl
from jax.experimental.pallas import tpu as pltpu
from jax.sharding import PartitionSpec as P

epsilon = 1e-06
MESH = pl.DeviceIdType.MESH
F32, BF16 = jnp.float32, jnp.bfloat16
CHUNKS = 4
TABLE = 16
COLUMNS = 256


def ring_of(groups, width):
    if width < 2 or groups % width or groups // width < 2:
        return list(range(groups))
    depth = groups // width
    cycle = []
    for x in range(width):
        column = range(1, depth) if x % 2 == 0 else range(depth - 1, 0, -1)
        cycle += [z * width + x for z in column]
    return cycle + [x for x in range(width - 1, -1, -1)]


def dot(a, b):
    return jnp.dot(a, b, preferred_element_type=F32)


def dot_nt(a, b):
    return lax.dot_general(a, b, (((1,), (1,)), ((), ())), preferred_element_type=F32)


def iota(shape, axis):
    return lax.broadcasted_iota(jnp.int32, shape, axis).astype(F32)


def layer_kernel(
    cfg,
    tokens_hbm,
    routes_ref,
    weights_ref,
    gain_ref,
    gate_hbm,
    up_hbm,
    down_hbm,
    sgate_hbm,
    sup_hbm,
    sdown_hbm,
    post_ref,
    out_ref,
    tok,
    xbuf,
    mbuf,
    gate,
    up,
    down,
    sgate,
    sup,
    sdown,
    rows,
    hits,
    lifts,
    parts,
    got1,
    sums,
    got2,
    hid,
    made,
    back,
    farb,
    mix,
    slotv,
    wv,
    rinv,
    rwt,
    earlier,
    eye,
    squares,
    token_sem,
    load_sem,
    gs,
    gr,
    ms,
    mr,
    rs,
    rr,
    s1s,
    s1r,
    s2s,
    s2r,
    s3s,
    s3r,
    s4s,
    s4r,
    ns,
    nr,
    credit,
):
    groups, members, experts, cap, fanout, ring, features = cfg
    count, width = out_ref.shape
    reach = groups // 2
    wide = members // 2
    units = gate.shape[2]
    share = units // members
    chunk = count // CHUNKS
    slots = experts * cap
    far = 2 * reach - 1
    middle = count // 2
    packed = mbuf.shape[1]

    group, me = lax.axis_index("ep"), lax.axis_index("tp")
    core, row = lax.rem(me, 2), lax.div(me, 2)
    ahead, behind = jnp.int32(0), jnp.int32(0)
    for i, place in enumerate(ring):
        here = group == place
        ahead = jnp.where(here, ring[(i + 1) % groups], ahead)
        behind = jnp.where(here, ring[(i - 1) % groups], behind)
    gather_to = ({"ep": ahead}, {"ep": behind})
    return_to = ({"ep": behind}, {"ep": ahead})
    partner = {"tp": row * 2 + 1 - core}

    def peer_row(d):
        return lax.rem(row + d, wide)

    def remote(src, dst, send, recv, to):
        return pltpu.make_async_remote_copy(
            src_ref=src, dst_ref=dst, send_sem=send, recv_sem=recv, device_id=to, device_id_type=MESH
        )

    barrier = pltpu.get_barrier_semaphore()
    for to in gather_to:
        pl.semaphore_signal(barrier, inc=1, device_id=to, device_id_type=MESH)
    for d in range(1, members):
        pl.semaphore_signal(
            barrier, inc=1, device_id={"tp": lax.rem(me + d, members)}, device_id_type=MESH
        )

    def piece(c):
        at = c * chunk
        return pl.ds(at if isinstance(c, int) else pl.multiple_of(at, chunk), chunk)

    token_loads = [
        pltpu.make_async_copy(tokens_hbm.at[piece(c)], tok.at[piece(c)], token_sem.at[c])
        for c in range(CHUNKS)
    ]
    for load in token_loads:
        load.start()
    loads = [
        pltpu.make_async_copy(src, dst, load_sem.at[i])
        for i, (src, dst) in enumerate(
            (
                (gate_hbm, gate),
                (up_hbm, up),
                (sgate_hbm, sgate),
                (sup_hbm, sup),
                (down_hbm, down),
                (sdown_hbm, sdown),
            )
        )
    ]

    def gather(d, step, c, first=False, last=False):
        src = 0 if first or isinstance(step, int) and step == 1 else 2 * step - 3 + d
        dst = far if last else 2 * step - 1 + d
        return remote(
            xbuf.at[src, piece(c)],
            xbuf.at[dst, piece(c)],
            gs.at[d, step, c],
            gr.at[d, step, c],
            gather_to[d],
        )

    def gather_meta(d, step, first=False):
        src = 0 if first or isinstance(step, int) and step == 1 else 2 * step - 3 + d
        return remote(
            mbuf.at[src], mbuf.at[2 * step - 1 + d], ms.at[d, step], mr.at[d, step], gather_to[d]
        )

    def half(d):
        return range(CHUNKS // 2) if d == 0 else range(CHUNKS // 2, CHUNKS)

    def scaled(c):
        xbuf[0, piece(c)] = (tok[piece(c)].astype(F32) * gain_ref[...]).astype(BF16)

    def diagonal(c):
        shape = (chunk, count)
        return iota(shape, 0) + float(c * chunk) == iota(shape, 1)

    def squares_of(c, value):
        column = jnp.sum(value * value, axis=1, keepdims=True)
        return jnp.sum(jnp.where(diagonal(c), column, 0.0), axis=0, keepdims=True)

    token_loads[0].wait()
    scaled(0)
    pl.semaphore_wait(barrier, 2 + members - 1)
    for d in range(2):
        gather(d, 1, 0, first=True).start()
    for c in range(1, CHUNKS):
        token_loads[c].wait()
    for load in loads:
        load.start()
    own_squares = jnp.zeros((1, count), F32)
    for c in range(CHUNKS):
        own_squares = own_squares + squares_of(c, tok[piece(c)].astype(F32))
    squares[0, me] = jnp.broadcast_to(own_squares, (8, count))

    def exchange_squares(which, meanwhile=lambda: None):
        copies = [
            remote(
                squares.at[which, me],
                squares.at[which, me],
                ns.at[which, d],
                nr.at[which, d],
                {"tp": lax.rem(me + d, members)},
            )
            for d in range(1, members)
        ]
        for copy in copies:
            copy.start()
        meanwhile()
        for copy in copies:
            copy.wait()
        total = squares[which, 0]
        for q in range(1, members):
            total = total + squares[which, q]
        return lax.rsqrt(total / features + epsilon)

    def finish_tokens():
        for c in range(1, CHUNKS):
            scaled(c)
        earlier[...] = jnp.where(iota(square, 0) < iota(square, 1), 1.0, 0.0).astype(BF16)
        eye[...] = jnp.where(iota(square, 0) == iota(square, 1), 1.0, 0.0).astype(BF16)

    square = (count, count)
    inverse_row = exchange_squares(0, finish_tokens)[0:1]
    high_weight = weights_ref[...].astype(BF16).astype(F32)
    high = inverse_row.astype(BF16).astype(F32)
    mid = (inverse_row - high).astype(BF16).astype(F32)
    mbuf[0] = jnp.concatenate(
        [
            routes_ref[...].astype(F32),
            high_weight,
            weights_ref[...] - high_weight,
            high,
            mid,
            inverse_row - high - mid,
        ]
        + [jnp.zeros((packed - 3 * fanout - 3, count), F32)],
        axis=0,
    ).astype(BF16)
    for d in range(2):
        gather_meta(d, 1, first=True).start()
        for c in range(1, CHUNKS):
            gather(d, 1, c, first=True).start()

    def poll(step, c):
        for d in range(2):
            if c == 0:
                gather_meta(d, step).wait_recv()

                @pl.when(step + 1 < reach + 1 - d)
                def _():
                    gather_meta(d, step + 1).start()

            gather(d, step, c).wait_recv()

            @pl.when(step + 1 < reach)
            def _():
                gather(d, step + 1, c).start()

            if c in half(d):

                @pl.when(step + 1 == reach)
                def _():
                    gather(d, reach, c, last=True).start()

    def tables(k):
        first = (group * experts).astype(F32)
        wanted = first + iota((TABLE, count), 0)
        present = jnp.zeros((TABLE, count), F32)
        weight = jnp.zeros((TABLE, count), F32)
        values = mbuf[k].astype(F32)
        for j in range(fanout):
            same = values[j : j + 1] == wanted
            present = present + jnp.where(same, 1.0, 0.0)
            exact = values[fanout + j : fanout + j + 1] + values[2 * fanout + j : 2 * fanout + j + 1]
            weight = weight + jnp.where(same, exact, 0.0)
        slot = dot(present.astype(BF16), earlier[...])
        slotv[k] = jnp.where(present > 0.0, slot, -1.0)
        wv[k] = weight
        at = 3 * fanout
        return values[at : at + 1] + values[at + 1 : at + 2] + values[at + 2 : at + 3]

    def row_values(turn, at, size, hit, inverse, weight):
        inv = jnp.sum(jnp.where(hit, inverse, 0.0), axis=1, keepdims=True)
        rinv[turn, at : at + size] = jnp.broadcast_to(inv, (size, 128))
        if weight is None:
            rwt[turn, at : at + size] = jnp.ones((size, 128), F32)
        else:
            value = jnp.sum(jnp.where(hit, weight, 0.0), axis=1, keepdims=True)
            rwt[turn, at : at + size] = jnp.broadcast_to(value, (size, 128))

    def prepare(turn, blocks, shared=False):
        n = len(blocks)
        for i, k in enumerate(blocks):
            inverse = tables(k)
            for e in range(experts):
                hit = iota((cap, count), 0) == slotv[k, e : e + 1]
                hits[i, e * cap : (e + 1) * cap] = jnp.where(hit, 1.0, 0.0).astype(BF16)
                row_values(turn, (e * n + i) * cap, cap, hit, inverse, wv[k, e : e + 1])
        if shared:
            for c in range(CHUNKS):
                row_values(turn, slots + c * chunk, chunk, diagonal(c), inverse, None)

    def put_parts(at, size, g, u):
        for q in range(members):
            parts[q, pl.ds(at, size), 0:share] = g[:, q * share : (q + 1) * share].astype(BF16)
            parts[q, pl.ds(at, size), share : 2 * share] = u[
                :, q * share : (q + 1) * share
            ].astype(BF16)

    def pick_rows(blocks, part=None):
        low, high = (0, count) if part is None else (part * middle, (part + 1) * middle)
        for i, k in enumerate(blocks):

            def pick(j, carry):
                at = pl.ds(pl.multiple_of(j * COLUMNS, COLUMNS), COLUMNS)
                picked = dot(hits[i, :, low:high], xbuf[k, low:high, at]).astype(BF16)
                for e in range(experts):
                    value = picked[e * cap : (e + 1) * cap]
                    if part == 1:
                        value = value + rows[e, i * cap : (i + 1) * cap, at]
                    rows[e, i * cap : (i + 1) * cap, at] = value
                return carry

            lax.fori_loop(0, width // COLUMNS, pick, 0)

    def project(e, n):
        taken = rows[e, 0 : n * cap]
        g, u = dot(taken, gate[e]), dot(taken, up[e])
        put_parts(pl.multiple_of(e * n * cap, n * cap), n * cap, g, u)

    def span(k, total):
        size = total // experts
        return pl.ds(k * size if isinstance(k, int) else pl.multiple_of(k * size, size), size)

    def core_copies(turn, k, total):
        return [
            remote(
                parts.at[y * 2 + 1 - core, span(k, total)],
                got1.at[turn, y, span(k, total)],
                s1s.at[turn, k, y],
                s1r.at[turn, k, y],
                partner,
            )
            for y in range(wide)
        ]

    def row_copies(turn, k, total):
        return [
            remote(
                sums.at[peer_row(d), span(k, total)],
                got2.at[turn, d - 1, span(k, total)],
                s2s.at[turn, k, d],
                s2r.at[turn, k, d],
                {"tp": peer_row(d) * 2 + core},
            )
            for d in range(1, wide)
        ]

    def hidden_row_copies(stage, k, total):
        turn = lax.rem(stage, 2)
        return [
            remote(
                hid.at[stage, me, span(k, total)],
                hid.at[stage, me, span(k, total)],
                s3s.at[turn, k, d],
                s3r.at[turn, k, d],
                {"tp": peer_row(d) * 2 + core},
            )
            for d in range(1, wide)
        ]

    def hidden_core_copies(stage, k, total):
        turn = lax.rem(stage, 2)
        return [
            remote(
                hid.at[stage, y * 2 + core, span(k, total)],
                hid.at[stage, y * 2 + core, span(k, total)],
                s4s.at[turn, k, y],
                s4r.at[turn, k, y],
                partner,
            )
            for y in range(wide)
        ]

    def start(copies):
        for copy in copies:
            copy.start()

    def wait(copies):
        for copy in copies:
            copy.wait()

    def add_core(turn, k, total):
        wait(core_copies(turn, k, total))
        at = span(k, total)
        for y in range(wide):
            mine = parts[y * 2 + core, at].astype(F32)
            sums[y, at] = (mine + got1[turn, y, at].astype(F32)).astype(BF16)
        start(row_copies(turn, k, total))

    def activate(stage, turn, k, total):
        wait(row_copies(turn, k, total))
        at = span(k, total)
        value = sums[row, at].astype(F32)
        for d in range(1, wide):
            value = value + got2[turn, d - 1, at].astype(F32)
        inv = rinv[turn, at, 0:share]
        g, u = value[:, 0:share] * inv, value[:, share : 2 * share] * inv
        hidden = g / (1.0 + jnp.exp(-g)) * u * rwt[turn, at, 0:share]
        hid[stage, me, at] = hidden.astype(BF16)
        start(hidden_row_copies(stage, k, total))

    def pass_hidden(stage, total):
        for k in range(experts):
            wait(hidden_row_copies(stage, k, total))
            start(hidden_core_copies(stage, k, total))

    def take_hidden(stage, total):
        for k in range(experts):
            wait(hidden_core_copies(stage, k, total))

    def send_parts(turn, n, total):
        def body(e, carry):
            project(e, n)
            start(core_copies(turn, e, total))

            @pl.when(e > 0)
            def _():
                add_core(turn, e - 1, total)

            return carry

        lax.fori_loop(0, experts, body, 0)
        add_core(turn, experts - 1, total)

    def columns(at, k):
        slot_column = dot_nt(eye[...], slotv[k].astype(BF16))
        for e in range(experts):
            hit = iota((count, cap), 1) == slot_column[:, e : e + 1]
            lifts[at, :, e * cap : (e + 1) * cap] = jnp.where(hit, 1.0, 0.0).astype(BF16)

    def produce(stage, e, n, first):
        at = pl.ds(pl.multiple_of(e * n * cap, n * cap), n * cap)
        taken = jnp.concatenate([hid[stage, q, at] for q in range(members)], axis=1)
        result = dot(taken, down[e]).astype(BF16)
        for i in range(n):
            made[first + i, pl.ds(pl.multiple_of(e * cap, cap), cap)] = result[
                i * cap : (i + 1) * cap
            ]

    def produce_all(stage, n, first):
        def body(e, carry):
            produce(stage, e, n, first)
            return carry

        lax.fori_loop(0, experts, body, 0)

    def scatter(i, low, high, put):
        def tile(j, carry):
            at = pl.ds(pl.multiple_of(j * COLUMNS, COLUMNS), COLUMNS)
            put(at, dot(lifts[i, low:high], made[i, :, at]))
            return carry

        lax.fori_loop(0, width // COLUMNS, tile, 0)

    first_rows = slots + count
    pair_rows = 2 * slots

    prepare(0, [0], True)
    for i in range(4):
        loads[i].wait()
    pick_rows([0])

    def own_rows(e, carry):
        project(e, 1)
        return carry

    lax.fori_loop(0, experts, own_rows, 0)

    def shared_rows(c, carry):
        taken = xbuf[0, piece(c)]
        g, u = dot(taken, sgate[...]), dot(taken, sup[...])
        put_parts(pl.multiple_of(slots + c * chunk, 32), chunk, g, u)
        return carry

    lax.fori_loop(0, CHUNKS, shared_rows, 0)
    for k in range(experts):
        start(core_copies(0, k, first_rows))
    for k in range(experts):
        add_core(0, k, first_rows)
    poll(1, 0)
    prepare(1, [1, 2])
    for k in range(experts):
        activate(0, 0, k, first_rows)
        if k == 0:
            poll(1, 1)
            pick_rows([1, 2], 0)
        if k == experts - 2:
            poll(1, 2)
    poll(1, 3)

    def run_stage(s, carry):
        turn = lax.rem(s, 2)

        @pl.when(s == 2)
        def _():
            take_hidden(0, first_rows)

        @pl.when(s > 2)
        def _():
            take_hidden(s - 2, pair_rows)

        pick_rows([2 * s - 1, 2 * s], 1)
        send_parts(turn, 2, pair_rows)
        @pl.when(s == 1)
        def _():
            pass_hidden(0, first_rows)

        @pl.when(s > 1)
        def _():
            pass_hidden(s - 1, pair_rows)

        def more(c):
            @pl.when(s + 1 < reach)
            def _():
                poll(s + 1, c)

        more(0)

        @pl.when(s + 1 < reach)
        def _():
            prepare(1 - turn, [2 * s + 1, 2 * s + 2])

        @pl.when(s + 1 == reach)
        def _():
            gather_meta(0, reach).wait_recv()
            prepare(1 - turn, [far])

        for k in range(experts):
            activate(s, turn, k, pair_rows)
            if k == 0:
                more(1)

                @pl.when(s + 1 < reach)
                def _():
                    pick_rows([2 * s + 1, 2 * s + 2], 0)

            if k == experts - 2:
                more(2)
        more(3)
        return carry

    lax.fori_loop(1, reach, run_stage, 0)

    last, spare = reach - 1, reach % 2
    take_hidden(reach - 2, pair_rows if reach > 2 else first_rows)
    for d in range(2):
        for c in half(d):
            gather(d, reach, c, last=True).wait_recv()
    pick_rows([far])
    send_parts(spare, 1, slots)
    columns(0, 2 * last - 1)
    columns(1, 2 * last)
    loads[4].wait()
    for k in range(experts):
        wait(hidden_row_copies(last, k, pair_rows))
        start(hidden_core_copies(last, k, pair_rows))
        if k > 0:
            wait(hidden_core_copies(last, k - 1, pair_rows))
            produce(last, k - 1, 2, 0)

    def sent(step, carry):
        for d in range(2):
            for c in range(CHUNKS):
                gather(d, step, c).wait_send()
            gather_meta(d, step).wait_send()
        return carry

    for d in range(2):
        for c in range(CHUNKS):
            gather(d, 1, c, first=True).wait_send()
        gather_meta(d, 1, first=True).wait_send()
        for c in half(d):
            gather(d, reach, c, last=True).wait_send()
    lax.fori_loop(2, reach, sent, 0)
    gather_meta(0, reach).wait_send()
    pl.semaphore_signal(credit.at[1], inc=1, device_id=return_to[0], device_id_type=MESH)
    pl.semaphore_signal(credit.at[0], inc=1, device_id=return_to[1], device_id_type=MESH)
    wait(hidden_core_copies(last, experts - 1, pair_rows))
    produce(last, experts - 1, 2, 0)

    def give(d, step, c, source):
        return remote(
            source.at[piece(c)],
            xbuf.at[2 * step - 1 + d, piece(c)],
            rs.at[d, step, c],
            rr.at[d, step, c],
            return_to[d],
        )

    def into(side, i, low, high):
        def put(at, value):
            back[side, i, low:high, at] = value.astype(BF16)

        return put

    side = last % 2
    top = back.at[side]
    order = [list(half(1)) + list(half(0)), list(half(0)) + list(half(1))]
    for d in range(2):
        low = middle if d == 0 else 0
        scatter(d, low, low + middle, into(side, d, low, low + middle))
        pl.semaphore_wait(credit.at[d], 1)
        for j in range(CHUNKS // 2):
            give(d, 2, order[d][j], top.at[d]).start()

    for k in range(experts):
        activate(reach, spare, k, slots)
    columns(2, far)
    for d in range(2):
        low = 0 if d == 0 else middle
        scatter(d, low, low + middle, into(side, d, low, low + middle))
    for k in range(experts):
        wait(hidden_row_copies(reach, k, slots))
        start(hidden_core_copies(reach, k, slots))
        if k > 0:
            wait(hidden_core_copies(reach, k - 1, slots))
            produce(reach, k - 1, 1, 2)
    wait(hidden_core_copies(reach, experts - 1, slots))
    produce(reach, experts - 1, 1, 2)

    def put_far(at, value):
        farb[:, at] = value.astype(BF16)

    scatter(2, 0, count, put_far)
    for j in range(CHUNKS // 2):
        for d in range(2):
            give(d, 1, order[d][CHUNKS // 2 + j], farb).start()

    def ready(s):
        produce_all(s, 2, 0)
        for i in range(2):
            columns(i, 2 * s - 1 + i)
            scatter(i, 0, count, into(lax.rem(s, 2), i, 0, count))

    if reach > 2:
        ready(reach - 2)

    def merge(d, step, c, source):
        give(d, step - 1, c, source).wait_recv()
        own = source[piece(c)].astype(F32)
        source[piece(c)] = (own + xbuf[2 * step - 3 + d, piece(c)].astype(F32)).astype(BF16)
        give(d, step, c, source).start()

    for j in range(CHUNKS // 2):
        for d in range(2):
            merge(d, 2, order[d][CHUNKS // 2 + j], top.at[d])

    for d in range(2):
        for c in half(d):
            give(d, 1, c, farb).wait_send()

    def returning(step, carry):
        s = reach + 1 - step
        now = back.at[lax.rem(s, 2)]
        for j in range(CHUNKS):
            for d in range(2):
                merge(d, step, order[d][j], now.at[d])
        for d in range(2):
            for c in range(CHUNKS):
                give(d, step - 1, c, back.at[lax.rem(s + 1, 2), d]).wait_send()

        @pl.when(s > 1)
        def _():
            ready(s - 1)

        return carry

    lax.fori_loop(3, reach + 1, returning, 0)

    loads[5].wait()

    def put_own(at, value):
        taken = jnp.concatenate(
            [hid[0, q, slots : slots + count] for q in range(members)], axis=1
        )
        mix[:, at] = value + dot(taken, sdown[:, at])

    produce_all(0, 1, 0)
    columns(0, 0)
    scatter(0, 0, count, put_own)
    taken_chunks = [0] * CHUNKS
    total = jnp.zeros((1, count), F32)
    for j in range(CHUNKS):
        for d in range(2):
            c = order[d][j]
            give(d, reach, c, back.at[1, d]).wait_recv()
            value = mix[piece(c)] + xbuf[2 * reach - 1 + d, piece(c)].astype(F32)
            mix[piece(c)] = value
            taken_chunks[c] += 1
            if taken_chunks[c] == 2:
                total = total + squares_of(c, value)
    squares[1, me] = jnp.broadcast_to(total, (8, count))
    scale = exchange_squares(1)[0:1]
    for c in range(CHUNKS):
        column = jnp.sum(jnp.where(diagonal(c), scale, 0.0), axis=1, keepdims=True)
        out_ref[piece(c)] = (mix[piece(c)] * column * post_ref[...]).astype(BF16)
    for d in range(2):
        for c in range(CHUNKS):
            give(d, reach, c, back.at[1, d]).wait_send()


def per_device(
    tokens,
    routes,
    route_weights,
    pre_gain,
    expert_gate,
    expert_up,
    expert_down,
    shared_gate,
    shared_up,
    shared_down,
    post_gain,
):
    members, groups = lax.axis_size("tp"), lax.axis_size("ep")
    count, width = tokens.shape
    fanout = routes.shape[1]
    experts, _, units = expert_gate.shape
    cap = 2 * count * fanout // (experts * groups)
    ring = tuple(ring_of(groups, members // 2))
    reach, wide = groups // 2, members // 2
    slots = experts * cap
    most = max(2 * slots, slots + count)
    share = units // members
    cfg = (groups, members, experts, cap, fanout, ring, float(width * members))

    vmem = pl.BlockSpec(memory_space=pltpu.VMEM)
    anywhere = pl.BlockSpec(memory_space=pl.ANY)
    dma = pltpu.SemaphoreType.DMA
    steps = reach + 1
    return pl.pallas_call(
        functools.partial(layer_kernel, cfg),
        out_shape=jax.ShapeDtypeStruct((count, width), BF16),
        in_specs=[anywhere, vmem, vmem, vmem] + [anywhere] * 6 + [vmem],
        out_specs=vmem,
        scratch_shapes=[
            pltpu.VMEM((count, width), BF16),
            pltpu.VMEM((groups + 1, count, width), BF16),
            pltpu.VMEM((groups, -(-(3 * fanout + 3) // 16) * 16, count), BF16),
            pltpu.VMEM(expert_gate.shape, BF16),
            pltpu.VMEM(expert_up.shape, BF16),
            pltpu.VMEM(expert_down.shape, BF16),
            pltpu.VMEM(shared_gate.shape, BF16),
            pltpu.VMEM(shared_up.shape, BF16),
            pltpu.VMEM(shared_down.shape, BF16),
            pltpu.VMEM((experts, 2 * cap, width), BF16),
            pltpu.VMEM((2, slots, count), BF16),
            pltpu.VMEM((3, count, slots), BF16),
            pltpu.VMEM((members, most, 2 * share), BF16),
            pltpu.VMEM((2, wide, most, 2 * share), BF16),
            pltpu.VMEM((wide, most, 2 * share), BF16),
            pltpu.VMEM((2, wide - 1, most, 2 * share), BF16),
            pltpu.VMEM((reach + 1, members, most, share), BF16),
            pltpu.VMEM((3, slots, width), BF16),
            pltpu.VMEM((2, 2, count, width), BF16),
            pltpu.VMEM((count, width), BF16),
            pltpu.VMEM((count, width), F32),
            pltpu.VMEM((groups, TABLE, count), F32),
            pltpu.VMEM((groups, TABLE, count), F32),
            pltpu.VMEM((2, most, 128), F32),
            pltpu.VMEM((2, most, 128), F32),
            pltpu.VMEM((count, count), BF16),
            pltpu.VMEM((count, count), BF16),
            pltpu.VMEM((2, members, 8, count), F32),
            dma((CHUNKS,)),
            dma((6,)),
            dma((2, steps, CHUNKS)),
            dma((2, steps, CHUNKS)),
            dma((2, steps)),
            dma((2, steps)),
            dma((2, steps, CHUNKS)),
            dma((2, steps, CHUNKS)),
            dma((2, experts, wide)),
            dma((2, experts, wide)),
            dma((2, experts, wide)),
            dma((2, experts, wide)),
            dma((2, experts, wide)),
            dma((2, experts, wide)),
            dma((2, experts, wide)),
            dma((2, experts, wide)),
            dma((2, members)),
            dma((2, members)),
            pltpu.SemaphoreType.REGULAR((2,)),
        ],
        compiler_params=pltpu.CompilerParams(
            collective_id=0, has_side_effects=True, vmem_limit_bytes=67043328
        ),
        name="layer",
    )(
        tokens,
        routes.T,
        route_weights.T,
        pre_gain[None, :],
        expert_gate,
        expert_up,
        expert_down,
        shared_gate,
        shared_up,
        shared_down,
        post_gain[None, :],
    )


def solution(mesh):
    in_specs = (
        P("ep", "tp"),
        P("ep", None),
        P("ep", None),
        P("tp"),
        P("ep", "tp", None),
        P("ep", "tp", None),
        P("ep", None, "tp"),
        P("tp", None),
        P("tp", None),
        P(None, "tp"),
        P("tp"),
    )
    return jax.shard_map(
        per_device, mesh=mesh, in_specs=in_specs, out_specs=P("ep", "tp"), check_vma=False
    )
```

time: 206 us -> 195 us (0.947)
  Pallas kernels: 202 us -> 193 us
    pallas_call x1, Pallas kernels: 202 us -> 193 us  [per_device(): pl.pallas_call(functools.partial(layer_kernel, cfg), out_shape=jax.ShapeD...]
where the time goes in v1:
time: 195 us
  Pallas kernels  193 us (99%)
  local copies, waits for them, and re-layouts  2.26 us (1%)
    pallas_call x1, Pallas kernels, per_device(): pl.pallas_call(functools.partial(layer_kernel, cfg), out_shape=jax.ShapeD...  193 us

profile of v1, /device:TPU:0, one launch (start us, length us, event | category | flops | bytes accessed | tf_op | source)
XLA Modules:
  0.0 195.1 jit_solution(6169841575212091738)
XLA Ops:
  0.0 192.9 %layer.1 = bf16[512,1024]{1,0:T(8,128)(2,1)} custom-call(bf16[512,1024]{1,0:T(8,128)(2,1)} %tokens_hbm.1, s32[4,512]{1,0:T(4,128)} %bitcast.4, f32[4,512]{1,0:T(4,128)} %bitcast.5, f32[1,1024]{1,0:T(1,128)} %bitcast.6, bf16[4,1024,512]{2,1,0:T(8,128)(2,1)} %gate_hbm.1, bf16[4,1024,512]{2,1,0:T(8,128)(2,1)} %up_hbm.1, bf16[4,512,1024]{2,1,0:T(8,128)(2,1)} %down_hbm.1, ...), custom_call_target="tpu_custom_call" | custom-call | tf_op jit(solution)/shard_map/layer/pallas_call | solution.py:758
  192.9 2.3 %copy.13 = bf16[512,1024]{1,0:T(8,128)(2,1)} copy(bf16[512,1024]{1,0:T(8,128)(2,1)} %layer.1) | data formatting | bytes 2097152

commit v2 on v1

--- a/solution.py
+++ b/solution.py
@@ -50,8 +50,8 @@
     sgate_hbm,
     sup_hbm,
     sdown_hbm,
-    post_ref,
-    out_ref,
+    mixed_hbm,
+    scale_ref,
     tok,
     xbuf,
     mbuf,
@@ -87,7 +87,6 @@
     ms,
     mr,
     rs,
-    rr,
     s1s,
     s1r,
     s2s,
@@ -101,7 +100,7 @@
     credit,
 ):
     groups, members, experts, cap, fanout, ring, features = cfg
-    count, width = out_ref.shape
+    count, width = mixed_hbm.shape
     reach = groups // 2
     wide = members // 2
     units = gate.shape[2]
@@ -169,16 +168,19 @@
         return remote(
             xbuf.at[src, piece(c)],
             xbuf.at[dst, piece(c)],
-            gs.at[d, step, c],
-            gr.at[d, step, c],
+            gs.at[d, 1 if last else 0],
+            gr.at[d, step - 1, c],
             gather_to[d],
         )
 
     def gather_meta(d, step, first=False):
         src = 0 if first or isinstance(step, int) and step == 1 else 2 * step - 3 + d
         return remote(
-            mbuf.at[src], mbuf.at[2 * step - 1 + d], ms.at[d, step], mr.at[d, step], gather_to[d]
+            mbuf.at[src], mbuf.at[2 * step - 1 + d], ms.at[d], mr.at[d, step - 1], gather_to[d]
         )
+
+    def sent(same, sem):
+        remote(same, same, sem, sem, partner).wait_send()
 
     def half(d):
         return range(CHUNKS // 2) if d == 0 else range(CHUNKS // 2, CHUNKS)
@@ -213,8 +215,8 @@
             remote(
                 squares.at[which, me],
                 squares.at[which, me],
-                ns.at[which, d],
-                nr.at[which, d],
+                ns.at[d - 1],
+                nr.at[d - 1],
                 {"tp": lax.rem(me + d, members)},
             )
             for d in range(1, members)
@@ -318,8 +320,8 @@
 
     def put_parts(at, size, g, u):
         for q in range(members):
-            parts[q, pl.ds(at, size), 0:share] = g[:, q * share : (q + 1) * share].astype(BF16)
-            parts[q, pl.ds(at, size), share : 2 * share] = u[
+            parts[q // 2, q % 2, pl.ds(at, size), 0:share] = g[:, q * share : (q + 1) * share].astype(BF16)
+            parts[q // 2, q % 2, pl.ds(at, size), share : 2 * share] = u[
                 :, q * share : (q + 1) * share
             ].astype(BF16)
 
@@ -331,13 +333,17 @@
                 at = pl.ds(pl.multiple_of(j * COLUMNS, COLUMNS), COLUMNS)
                 picked = dot(hits[i, :, low:high], xbuf[k, low:high, at]).astype(BF16)
                 for e in range(experts):
-                    value = picked[e * cap : (e + 1) * cap]
-                    if part == 1:
-                        value = value + rows[e, i * cap : (i + 1) * cap, at]
-                    rows[e, i * cap : (i + 1) * cap, at] = value
+                    rows[e, i * cap : (i + 1) * cap, at] = picked[e * cap : (e + 1) * cap]
                 return carry
 
             lax.fori_loop(0, width // COLUMNS, pick, 0)
+
+    def pick_more(e, blocks):
+        own = pl.ds(pl.multiple_of(e * cap, cap), cap)
+        for i, k in enumerate(blocks):
+            picked = dot(hits[i, own, middle:], xbuf[k, middle:]).astype(BF16)
+            at = slice(i * cap, (i + 1) * cap)
+            rows[e, at] = rows[e, at] + picked
 
     def project(e, n):
         taken = rows[e, 0 : n * cap]
@@ -351,13 +357,12 @@
     def core_copies(turn, k, total):
         return [
             remote(
-                parts.at[y * 2 + 1 - core, span(k, total)],
-                got1.at[turn, y, span(k, total)],
-                s1s.at[turn, k, y],
-                s1r.at[turn, k, y],
+                parts.at[:, 1 - core, span(k, total)],
+                got1.at[turn, :, span(k, total)],
+                s1s.at[k],
+                s1r.at[turn, k],
                 partner,
             )
-            for y in range(wide)
         ]
 
     def row_copies(turn, k, total):
@@ -365,8 +370,8 @@
             remote(
                 sums.at[peer_row(d), span(k, total)],
                 got2.at[turn, d - 1, span(k, total)],
-                s2s.at[turn, k, d],
-                s2r.at[turn, k, d],
+                s2s.at[k, d - 1],
+                s2r.at[turn, k, d - 1],
                 {"tp": peer_row(d) * 2 + core},
             )
             for d in range(1, wide)
@@ -376,10 +381,10 @@
         turn = lax.rem(stage, 2)
         return [
             remote(
-                hid.at[stage, me, span(k, total)],
-                hid.at[stage, me, span(k, total)],
-                s3s.at[turn, k, d],
-                s3r.at[turn, k, d],
+                hid.at[stage, row, core, span(k, total)],
+                hid.at[stage, row, core, span(k, total)],
+                s3s.at[turn, k, d - 1],
+                s3r.at[turn, k, d - 1],
                 {"tp": peer_row(d) * 2 + core},
             )
             for d in range(1, wide)
@@ -389,13 +394,12 @@
         turn = lax.rem(stage, 2)
         return [
             remote(
-                hid.at[stage, y * 2 + core, span(k, total)],
-                hid.at[stage, y * 2 + core, span(k, total)],
-                s4s.at[turn, k, y],
-                s4r.at[turn, k, y],
+                hid.at[stage, :, core, span(k, total)],
+                hid.at[stage, :, core, span(k, total)],
+                s4s.at[turn, k],
+                s4r.at[turn, k],
                 partner,
             )
-            for y in range(wide)
         ]
 
     def start(copies):
@@ -410,7 +414,7 @@
         wait(core_copies(turn, k, total))
         at = span(k, total)
         for y in range(wide):
-            mine = parts[y * 2 + core, at].astype(F32)
+            mine = parts[y, core, at].astype(F32)
             sums[y, at] = (mine + got1[turn, y, at].astype(F32)).astype(BF16)
         start(row_copies(turn, k, total))
 
@@ -423,7 +427,7 @@
         inv = rinv[turn, at, 0:share]
         g, u = value[:, 0:share] * inv, value[:, share : 2 * share] * inv
         hidden = g / (1.0 + jnp.exp(-g)) * u * rwt[turn, at, 0:share]
-        hid[stage, me, at] = hidden.astype(BF16)
+        hid[stage, row, core, at] = hidden.astype(BF16)
         start(hidden_row_copies(stage, k, total))
 
     def pass_hidden(stage, total):
@@ -435,8 +439,10 @@
         for k in range(experts):
             wait(hidden_core_copies(stage, k, total))
 
-    def send_parts(turn, n, total):
+    def send_parts(turn, n, total, more=None):
         def body(e, carry):
+            if more is not None:
+                pick_more(e, more)
             project(e, n)
             start(core_copies(turn, e, total))
 
@@ -457,7 +463,7 @@
 
     def produce(stage, e, n, first):
         at = pl.ds(pl.multiple_of(e * n * cap, n * cap), n * cap)
-        taken = jnp.concatenate([hid[stage, q, at] for q in range(members)], axis=1)
+        taken = jnp.concatenate([hid[stage, q // 2, q % 2, at] for q in range(members)], axis=1)
         result = dot(taken, down[e]).astype(BF16)
         for i in range(n):
             made[first + i, pl.ds(pl.multiple_of(e * cap, cap), cap)] = result[
@@ -526,8 +532,7 @@
         def _():
             take_hidden(s - 2, pair_rows)
 
-        pick_rows([2 * s - 1, 2 * s], 1)
-        send_parts(turn, 2, pair_rows)
+        send_parts(turn, 2, pair_rows, [2 * s - 1, 2 * s])
         @pl.when(s == 1)
         def _():
             pass_hidden(0, first_rows)
@@ -551,6 +556,9 @@
         def _():
             gather_meta(0, reach).wait_recv()
             prepare(1 - turn, [far])
+            columns(0, 2 * s - 1)
+            columns(1, 2 * s)
+            columns(2, far)
 
         for k in range(experts):
             activate(s, turn, k, pair_rows)
@@ -575,42 +583,27 @@
             gather(d, reach, c, last=True).wait_recv()
     pick_rows([far])
     send_parts(spare, 1, slots)
-    columns(0, 2 * last - 1)
-    columns(1, 2 * last)
+    pass_hidden(last, pair_rows)
     loads[4].wait()
-    for k in range(experts):
-        wait(hidden_row_copies(last, k, pair_rows))
-        start(hidden_core_copies(last, k, pair_rows))
-        if k > 0:
-            wait(hidden_core_copies(last, k - 1, pair_rows))
-            produce(last, k - 1, 2, 0)
-
-    def sent(step, carry):
-        for d in range(2):
-            for c in range(CHUNKS):
-                gather(d, step, c).wait_send()
-            gather_meta(d, step).wait_send()
-        return carry
+    for k in range(experts - 1):
+        wait(hidden_core_copies(last, k, pair_rows))
+        produce(last, k, 2, 0)
 
     for d in range(2):
-        for c in range(CHUNKS):
-            gather(d, 1, c, first=True).wait_send()
-        gather_meta(d, 1, first=True).wait_send()
-        for c in half(d):
-            gather(d, reach, c, last=True).wait_send()
-    lax.fori_loop(2, reach, sent, 0)
-    gather_meta(0, reach).wait_send()
+        sent(xbuf.at[0 : reach - 1], gs.at[d, 0])
+        sent(xbuf.at[0, 0:middle], gs.at[d, 1])
+        sent(mbuf.at[0 : reach - d], ms.at[d])
     pl.semaphore_signal(credit.at[1], inc=1, device_id=return_to[0], device_id_type=MESH)
     pl.semaphore_signal(credit.at[0], inc=1, device_id=return_to[1], device_id_type=MESH)
     wait(hidden_core_copies(last, experts - 1, pair_rows))
     produce(last, experts - 1, 2, 0)
 
-    def give(d, step, c, source):
+    def give(d, step, c, source, far_block=False):
         return remote(
             source.at[piece(c)],
             xbuf.at[2 * step - 1 + d, piece(c)],
-            rs.at[d, step, c],
-            rr.at[d, step, c],
+            rs.at[d, 2 if far_block else lax.rem(step, 2)],
+            gr.at[d, step - 1, c],
             return_to[d],
         )
 
@@ -632,7 +625,6 @@
 
     for k in range(experts):
         activate(reach, spare, k, slots)
-    columns(2, far)
     for d in range(2):
         low = 0 if d == 0 else middle
         scatter(d, low, low + middle, into(side, d, low, low + middle))
@@ -651,7 +643,7 @@
     scatter(2, 0, count, put_far)
     for j in range(CHUNKS // 2):
         for d in range(2):
-            give(d, 1, order[d][CHUNKS // 2 + j], farb).start()
+            give(d, 1, order[d][CHUNKS // 2 + j], farb, True).start()
 
     def ready(s):
         produce_all(s, 2, 0)
@@ -673,8 +665,7 @@
             merge(d, 2, order[d][CHUNKS // 2 + j], top.at[d])
 
     for d in range(2):
-        for c in half(d):
-            give(d, 1, c, farb).wait_send()
+        sent(farb.at[0:middle], rs.at[d, 2])
 
     def returning(step, carry):
         s = reach + 1 - step
@@ -683,8 +674,7 @@
             for d in range(2):
                 merge(d, step, order[d][j], now.at[d])
         for d in range(2):
-            for c in range(CHUNKS):
-                give(d, step - 1, c, back.at[lax.rem(s + 1, 2), d]).wait_send()
+            sent(back.at[0, d], rs.at[d, lax.rem(step - 1, 2)])
 
         @pl.when(s > 1)
         def _():
@@ -698,13 +688,17 @@
 
     def put_own(at, value):
         taken = jnp.concatenate(
-            [hid[0, q, slots : slots + count] for q in range(members)], axis=1
+            [hid[0, q // 2, q % 2, slots : slots + count] for q in range(members)], axis=1
         )
         mix[:, at] = value + dot(taken, sdown[:, at])
 
     produce_all(0, 1, 0)
     columns(0, 0)
     scatter(0, 0, count, put_own)
+    stores = [
+        pltpu.make_async_copy(tok.at[piece(c)], mixed_hbm.at[piece(c)], token_sem.at[c])
+        for c in range(CHUNKS)
+    ]
     taken_chunks = [0] * CHUNKS
     total = jnp.zeros((1, count), F32)
     for j in range(CHUNKS):
@@ -712,18 +706,26 @@
             c = order[d][j]
             give(d, reach, c, back.at[1, d]).wait_recv()
             value = mix[piece(c)] + xbuf[2 * reach - 1 + d, piece(c)].astype(F32)
-            mix[piece(c)] = value
             taken_chunks[c] += 1
-            if taken_chunks[c] == 2:
+            if taken_chunks[c] == 1:
+                mix[piece(c)] = value
+            else:
+                tok[piece(c)] = value.astype(BF16)
+                stores[c].start()
                 total = total + squares_of(c, value)
     squares[1, me] = jnp.broadcast_to(total, (8, count))
-    scale = exchange_squares(1)[0:1]
+    scale_ref[...] = exchange_squares(1)
     for c in range(CHUNKS):
-        column = jnp.sum(jnp.where(diagonal(c), scale, 0.0), axis=1, keepdims=True)
-        out_ref[piece(c)] = (mix[piece(c)] * column * post_ref[...]).astype(BF16)
+        stores[c].wait()
     for d in range(2):
-        for c in range(CHUNKS):
-            give(d, reach, c, back.at[1, d]).wait_send()
+        sent(back.at[0, d], rs.at[d, reach % 2])
+
+
+def finish_kernel(mixed_ref, scale_ref, post_ref, out_ref):
+    shape = (mixed_ref.shape[0],) * 2
+    same = iota(shape, 0) == iota(shape, 1)
+    column = jnp.sum(jnp.where(same, scale_ref[0:1], 0.0), axis=1, keepdims=True)
+    out_ref[...] = (mixed_ref[...].astype(F32) * column * post_ref[...]).astype(BF16)
 
 
 def per_device(
@@ -754,12 +756,14 @@
     vmem = pl.BlockSpec(memory_space=pltpu.VMEM)
     anywhere = pl.BlockSpec(memory_space=pl.ANY)
     dma = pltpu.SemaphoreType.DMA
-    steps = reach + 1
-    return pl.pallas_call(
+    mixed, scale = pl.pallas_call(
         functools.partial(layer_kernel, cfg),
-        out_shape=jax.ShapeDtypeStruct((count, width), BF16),
-        in_specs=[anywhere, vmem, vmem, vmem] + [anywhere] * 6 + [vmem],
-        out_specs=vmem,
+        out_shape=[
+            jax.ShapeDtypeStruct((count, width), BF16),
+            jax.ShapeDtypeStruct((8, count), F32),
+        ],
+        in_specs=[anywhere, vmem, vmem, vmem] + [anywhere] * 6,
+        out_specs=[anywhere, vmem],
         scratch_shapes=[
             pltpu.VMEM((count, width), BF16),
             pltpu.VMEM((groups + 1, count, width), BF16),
@@ -773,11 +777,11 @@
             pltpu.VMEM((experts, 2 * cap, width), BF16),
             pltpu.VMEM((2, slots, count), BF16),
             pltpu.VMEM((3, count, slots), BF16),
-            pltpu.VMEM((members, most, 2 * share), BF16),
+            pltpu.VMEM((wide, 2, most, 2 * share), BF16),
             pltpu.VMEM((2, wide, most, 2 * share), BF16),
             pltpu.VMEM((wide, most, 2 * share), BF16),
             pltpu.VMEM((2, wide - 1, most, 2 * share), BF16),
-            pltpu.VMEM((reach + 1, members, most, share), BF16),
+            pltpu.VMEM((reach + 1, wide, 2, most, share), BF16),
             pltpu.VMEM((3, slots, width), BF16),
             pltpu.VMEM((2, 2, count, width), BF16),
             pltpu.VMEM((count, width), BF16),
@@ -791,22 +795,21 @@
             pltpu.VMEM((2, members, 8, count), F32),
             dma((CHUNKS,)),
             dma((6,)),
-            dma((2, steps, CHUNKS)),
-            dma((2, steps, CHUNKS)),
-            dma((2, steps)),
-            dma((2, steps)),
-            dma((2, steps, CHUNKS)),
-            dma((2, steps, CHUNKS)),
-            dma((2, experts, wide)),
-            dma((2, experts, wide)),
-            dma((2, experts, wide)),
-            dma((2, experts, wide)),
-            dma((2, experts, wide)),
-            dma((2, experts, wide)),
-            dma((2, experts, wide)),
-            dma((2, experts, wide)),
-            dma((2, members)),
-            dma((2, members)),
+            dma((2, 2)),
+            dma((2, reach, CHUNKS)),
+            dma((2,)),
+            dma((2, reach)),
+            dma((2, 3)),
+            dma((experts,)),
+            dma((2, experts)),
+            dma((experts, wide - 1)),
+            dma((2, experts, wide - 1)),
+            dma((2, experts, wide - 1)),
+            dma((2, experts, wide - 1)),
+            dma((2, experts)),
+            dma((2, experts)),
+            dma((members - 1,)),
+            dma((members - 1,)),
             pltpu.SemaphoreType.REGULAR((2,)),
         ],
         compiler_params=pltpu.CompilerParams(
@@ -824,8 +827,20 @@
         shared_gate,
         shared_up,
         shared_down,
-        post_gain[None, :],
     )
+    block = count // 2
+    return pl.pallas_call(
+        finish_kernel,
+        grid=(2,),
+        in_specs=[
+            pl.BlockSpec((block, width), lambda c: (c, 0)),
+            pl.BlockSpec((8, block), lambda c: (0, c)),
+            pl.BlockSpec((1, width), lambda c: (0, 0)),
+        ],
+        out_specs=pl.BlockSpec((block, width), lambda c: (c, 0)),
+        out_shape=jax.ShapeDtypeStruct((count, width), BF16),
+        name="finish",
+    )(mixed, scale, post_gain[None, :])
 
 
 def solution(mesh):

time: 195 us -> 189 us (0.969)
  Pallas kernels: 193 us -> 189 us
  local copies, waits for them, and re-layouts: 2.26 us -> 0 us
    pallas_call x1 -> x2, Pallas kernels: 193 us -> 189 us  [the longest x1 187 us: per_device(): pl.pallas_call(functools.partial(layer_kernel, cfg), out_shape=[jax.Shape...]
    unnamed x1 -> x0, local copies, waits for them, and re-layouts: 2.26 us -> none
where the time goes in v2:
time: 189 us
  Pallas kernels  189 us (100%)
    pallas_call x1, Pallas kernels, per_device(): pl.pallas_call(functools.partial(layer_kernel, cfg), out_shape=[jax.Shape...  187 us

profile of v2, /device:TPU:0, one launch (start us, length us, event | category | flops | bytes accessed | tf_op | source)
XLA Modules:
  0.0 189.3 jit_solution(14391858621969315429)
XLA Ops:
  0.0 187.0 %layer.1 = (bf16[512,1024]{1,0:T(8,128)(2,1)}, f32[8,512]{1,0:T(8,128)}) custom-call(bf16[512,1024]{1,0:T(8,128)(2,1)} %tokens_hbm.1, s32[4,512]{1,0:T(4,128)} %bitcast.4, f32[4,512]{1,0:T(4,128)} %bitcast.5, f32[1,1024]{1,0:T(1,128)} %bitcast.7, bf16[4,1024,512]{2,1,0:T(8,128)(2,1)} %gate_hbm.1, bf16[4,1024,512]{2,1,0:T(8,128)(2,1)} %up_hbm.1, ...), custom_call_target="tpu_custom_call" | custom-call | tf_op jit(solution)/shard_map/layer/pallas_call | solution.py:759
  187.0 2.3 %finish.1 = bf16[512,1024]{1,0:T(8,128)(2,1)} custom-call(bf16[512,1024]{1,0:T(8,128)(2,1)} %get-tuple-element.7.mixed_ref, f32[8,512]{1,0:T(8,128)} %get-tuple-element.8.scale_ref, f32[1,1024]{1,0:T(1,128)} %bitcast.6), custom_call_target="tpu_custom_call" | custom-call | tf_op jit(solution)/shard_map/finish/pallas_call | solution.py:832

commit v3 on v2

--- a/solution.py
+++ b/solution.py
@@ -41,17 +41,22 @@
 def layer_kernel(
     cfg,
     tokens_hbm,
-    routes_ref,
-    weights_ref,
-    gain_ref,
+    routes_hbm,
+    weights_hbm,
+    gain_hbm,
+    post_hbm,
     gate_hbm,
     up_hbm,
     down_hbm,
     sgate_hbm,
     sup_hbm,
     sdown_hbm,
-    mixed_hbm,
+    mixed_ref,
     scale_ref,
+    routes_ref,
+    weights_ref,
+    gain_ref,
+    post_ref,
     tok,
     xbuf,
     mbuf,
@@ -80,6 +85,7 @@
     earlier,
     eye,
     squares,
+    small_sem,
     token_sem,
     load_sem,
     gs,
@@ -100,7 +106,7 @@
     credit,
 ):
     groups, members, experts, cap, fanout, ring, features = cfg
-    count, width = mixed_hbm.shape
+    count, width = mixed_ref.shape
     reach = groups // 2
     wide = members // 2
     units = gate.shape[2]
@@ -130,6 +136,28 @@
             src_ref=src, dst_ref=dst, send_sem=send, recv_sem=recv, device_id=to, device_id_type=MESH
         )
 
+    def piece(c):
+        at = c * chunk
+        return pl.ds(at if isinstance(c, int) else pl.multiple_of(at, chunk), chunk)
+
+    token_loads = [
+        pltpu.make_async_copy(tokens_hbm.at[piece(c)], tok.at[piece(c)], token_sem.at[c])
+        for c in range(CHUNKS)
+    ]
+    small_loads = [
+        pltpu.make_async_copy(src, dst, small_sem.at[i])
+        for i, (src, dst) in enumerate(
+            (
+                (gain_hbm, gain_ref),
+                (routes_hbm, routes_ref),
+                (weights_hbm, weights_ref),
+                (post_hbm, post_ref),
+            )
+        )
+    ]
+    small_loads[0].start()
+    for load in token_loads:
+        load.start()
     barrier = pltpu.get_barrier_semaphore()
     for to in gather_to:
         pl.semaphore_signal(barrier, inc=1, device_id=to, device_id_type=MESH)
@@ -138,15 +166,7 @@
             barrier, inc=1, device_id={"tp": lax.rem(me + d, members)}, device_id_type=MESH
         )
 
-    def piece(c):
-        at = c * chunk
-        return pl.ds(at if isinstance(c, int) else pl.multiple_of(at, chunk), chunk)
-
-    token_loads = [
-        pltpu.make_async_copy(tokens_hbm.at[piece(c)], tok.at[piece(c)], token_sem.at[c])
-        for c in range(CHUNKS)
-    ]
-    for load in token_loads:
+    for load in small_loads[1:]:
         load.start()
     loads = [
         pltpu.make_async_copy(src, dst, load_sem.at[i])
@@ -196,6 +216,7 @@
         column = jnp.sum(value * value, axis=1, keepdims=True)
         return jnp.sum(jnp.where(diagonal(c), column, 0.0), axis=0, keepdims=True)
 
+    small_loads[0].wait()
     token_loads[0].wait()
     scaled(0)
     pl.semaphore_wait(barrier, 2 + members - 1)
@@ -239,6 +260,8 @@
 
     square = (count, count)
     inverse_row = exchange_squares(0, finish_tokens)[0:1]
+    for load in small_loads[1:]:
+        load.wait()
     high_weight = weights_ref[...].astype(BF16).astype(F32)
     high = inverse_row.astype(BF16).astype(F32)
     mid = (inverse_row - high).astype(BF16).astype(F32)
@@ -616,11 +639,12 @@
     side = last % 2
     top = back.at[side]
     order = [list(half(1)) + list(half(0)), list(half(0)) + list(half(1))]
-    for d in range(2):
-        low = middle if d == 0 else 0
-        scatter(d, low, low + middle, into(side, d, low, low + middle))
-        pl.semaphore_wait(credit.at[d], 1)
-        for j in range(CHUNKS // 2):
+    for j in range(CHUNKS // 2):
+        for d in range(2):
+            low = order[d][j] * chunk
+            scatter(d, low, low + chunk, into(side, d, low, low + chunk))
+            if j == 0:
+                pl.semaphore_wait(credit.at[d], 1)
             give(d, 2, order[d][j], top.at[d]).start()
 
     for k in range(experts):
@@ -695,10 +719,6 @@
     produce_all(0, 1, 0)
     columns(0, 0)
     scatter(0, 0, count, put_own)
-    stores = [
-        pltpu.make_async_copy(tok.at[piece(c)], mixed_hbm.at[piece(c)], token_sem.at[c])
-        for c in range(CHUNKS)
-    ]
     taken_chunks = [0] * CHUNKS
     total = jnp.zeros((1, count), F32)
     for j in range(CHUNKS):
@@ -710,22 +730,19 @@
             if taken_chunks[c] == 1:
                 mix[piece(c)] = value
             else:
-                tok[piece(c)] = value.astype(BF16)
-                stores[c].start()
+                mixed_ref[piece(c)] = (value * post_ref[...]).astype(BF16)
                 total = total + squares_of(c, value)
     squares[1, me] = jnp.broadcast_to(total, (8, count))
     scale_ref[...] = exchange_squares(1)
-    for c in range(CHUNKS):
-        stores[c].wait()
     for d in range(2):
         sent(back.at[0, d], rs.at[d, reach % 2])
 
 
-def finish_kernel(mixed_ref, scale_ref, post_ref, out_ref):
+def finish_kernel(mixed_ref, scale_ref, out_ref):
     shape = (mixed_ref.shape[0],) * 2
     same = iota(shape, 0) == iota(shape, 1)
     column = jnp.sum(jnp.where(same, scale_ref[0:1], 0.0), axis=1, keepdims=True)
-    out_ref[...] = (mixed_ref[...].astype(F32) * column * post_ref[...]).astype(BF16)
+    out_ref[...] = (mixed_ref[...].astype(F32) * column).astype(BF16)
 
 
 def per_device(
@@ -759,12 +776,16 @@
     mixed, scale = pl.pallas_call(
         functools.partial(layer_kernel, cfg),
         out_shape=[
-            jax.ShapeDtypeStruct((count, width), BF16),
-            jax.ShapeDtypeStruct((8, count), F32),
+            pltpu.VMEM((count, width), BF16),
+            pltpu.VMEM((8, count), F32),
         ],
-        in_specs=[anywhere, vmem, vmem, vmem] + [anywhere] * 6,
-        out_specs=[anywhere, vmem],
+        in_specs=[anywhere] * 11,
+        out_specs=[vmem, vmem],
         scratch_shapes=[
+            pltpu.VMEM((fanout, count), routes.dtype),
+            pltpu.VMEM((fanout, count), F32),
+            pltpu.VMEM((1, width), F32),
+            pltpu.VMEM((1, width), F32),
             pltpu.VMEM((count, width), BF16),
             pltpu.VMEM((groups + 1, count, width), BF16),
             pltpu.VMEM((groups, -(-(3 * fanout + 3) // 16) * 16, count), BF16),
@@ -793,6 +814,7 @@
             pltpu.VMEM((count, count), BF16),
             pltpu.VMEM((count, count), BF16),
             pltpu.VMEM((2, members, 8, count), F32),
+            dma((4,)),
             dma((CHUNKS,)),
             dma((6,)),
             dma((2, 2)),
@@ -813,7 +835,7 @@
             pltpu.SemaphoreType.REGULAR((2,)),
         ],
         compiler_params=pltpu.CompilerParams(
-            collective_id=0, has_side_effects=True, vmem_limit_bytes=67043328
+            collective_id=0, has_side_effects=True, vmem_limit_bytes=66977792 - 2 * count * width - 32 * count
         ),
         name="layer",
     )(
@@ -821,6 +843,7 @@
         routes.T,
         route_weights.T,
         pre_gain[None, :],
+        post_gain[None, :],
         expert_gate,
         expert_up,
         expert_down,
@@ -828,6 +851,8 @@
         shared_up,
         shared_down,
     )
+    mixed = pltpu.with_memory_space_constraint(mixed, pltpu.VMEM)
+    scale = pltpu.with_memory_space_constraint(scale, pltpu.VMEM)
     block = count // 2
     return pl.pallas_call(
         finish_kernel,
@@ -835,12 +860,11 @@
         in_specs=[
             pl.BlockSpec((block, width), lambda c: (c, 0)),
             pl.BlockSpec((8, block), lambda c: (0, c)),
-            pl.BlockSpec((1, width), lambda c: (0, 0)),
         ],
         out_specs=pl.BlockSpec((block, width), lambda c: (c, 0)),
         out_shape=jax.ShapeDtypeStruct((count, width), BF16),
         name="finish",
-    )(mixed, scale, post_gain[None, :])
+    )(mixed, scale)
 
 
 def solution(mesh):

time: 189 us -> 187 us (0.989)
  Pallas kernels: 189 us -> 187 us
where the time goes in v3:
time: 187 us
  Pallas kernels  187 us (100%)
    pallas_call x1, Pallas kernels, per_device(): pl.pallas_call(functools.partial(layer_kernel, cfg), out_shape=[pltpu.VME...  185 us

profile of v3, /device:TPU:0, one launch (start us, length us, event | category | flops | bytes accessed | tf_op | source)
XLA Modules:
  0.0 186.6 jit_solution(10466360144958942420)
XLA Ops:
  0.0 185.4 %layer.1 = (bf16[512,1024]{1,0:T(8,128)(2,1)S(1)}, f32[8,512]{1,0:T(8,128)S(1)}) custom-call(bf16[512,1024]{1,0:T(8,128)(2,1)} %tokens_hbm.1, s32[4,512]{1,0:T(4,128)} %bitcast.4, f32[4,512]{1,0:T(4,128)} %bitcast.5, f32[1,1024]{1,0:T(1,128)} %bitcast.6, f32[1,1024]{1,0:T(1,128)} %bitcast.7, bf16[4,1024,512]{2,1,0:T(8,128)(2,1)} %gate_hbm.1, ...), custom_call_target="tpu_custom_call" | custom-call | tf_op jit(solution)/shard_map/layer/pallas_call | solution.py:776
  185.4 1.2 finish.1

commit v4 on v3

--- a/solution.py
+++ b/solution.py
@@ -229,7 +229,7 @@
     own_squares = jnp.zeros((1, count), F32)
     for c in range(CHUNKS):
         own_squares = own_squares + squares_of(c, tok[piece(c)].astype(F32))
-    squares[0, me] = jnp.broadcast_to(own_squares, (8, count))
+    squares[0, me] = own_squares
 
     def exchange_squares(which, meanwhile=lambda: None):
         copies = [
@@ -259,7 +259,7 @@
         eye[...] = jnp.where(iota(square, 0) == iota(square, 1), 1.0, 0.0).astype(BF16)
 
     square = (count, count)
-    inverse_row = exchange_squares(0, finish_tokens)[0:1]
+    inverse_row = exchange_squares(0, finish_tokens)
     for load in small_loads[1:]:
         load.wait()
     high_weight = weights_ref[...].astype(BF16).astype(F32)
@@ -453,16 +453,19 @@
         hid[stage, row, core, at] = hidden.astype(BF16)
         start(hidden_row_copies(stage, k, total))
 
+    def pass_one(stage, k, total):
+        wait(hidden_row_copies(stage, k, total))
+        start(hidden_core_copies(stage, k, total))
+
     def pass_hidden(stage, total):
         for k in range(experts):
-            wait(hidden_row_copies(stage, k, total))
-            start(hidden_core_copies(stage, k, total))
+            pass_one(stage, k, total)
 
     def take_hidden(stage, total):
         for k in range(experts):
             wait(hidden_core_copies(stage, k, total))
 
-    def send_parts(turn, n, total, more=None):
+    def send_parts(turn, n, total, more=None, beside=None):
         def body(e, carry):
             if more is not None:
                 pick_more(e, more)
@@ -472,6 +475,8 @@
             @pl.when(e > 0)
             def _():
                 add_core(turn, e - 1, total)
+                if beside is not None:
+                    beside(e - 1)
 
             return carry
 
@@ -605,8 +610,8 @@
         for c in half(d):
             gather(d, reach, c, last=True).wait_recv()
     pick_rows([far])
-    send_parts(spare, 1, slots)
-    pass_hidden(last, pair_rows)
+    send_parts(spare, 1, slots, beside=lambda k: pass_one(last, k, pair_rows))
+    pass_one(last, experts - 1, pair_rows)
     loads[4].wait()
     for k in range(experts - 1):
         wait(hidden_core_copies(last, k, pair_rows))
@@ -732,8 +737,8 @@
             else:
                 mixed_ref[piece(c)] = (value * post_ref[...]).astype(BF16)
                 total = total + squares_of(c, value)
-    squares[1, me] = jnp.broadcast_to(total, (8, count))
-    scale_ref[...] = exchange_squares(1)
+    squares[1, me] = total
+    scale_ref[...] = jnp.broadcast_to(exchange_squares(1), (8, count))
     for d in range(2):
         sent(back.at[0, d], rs.at[d, reach % 2])
 
@@ -813,7 +818,7 @@
             pltpu.VMEM((2, most, 128), F32),
             pltpu.VMEM((count, count), BF16),
             pltpu.VMEM((count, count), BF16),
-            pltpu.VMEM((2, members, 8, count), F32),
+            pltpu.VMEM((2, members, 1, count), F32),
             dma((4,)),
             dma((CHUNKS,)),
             dma((6,)),

time: 187 us -> 185 us (0.989)
  Pallas kernels: 187 us -> 185 us
where the time goes in v4:
time: 185 us
  Pallas kernels  185 us (100%)
    pallas_call x1, Pallas kernels, per_device(): pl.pallas_call(functools.partial(layer_kernel, cfg), out_shape=[pltpu.VME...  184 us

profile of v4, /device:TPU:0, one launch (start us, length us, event | category | flops | bytes accessed | tf_op | source)
XLA Modules:
  0.0 185.3 jit_solution(14023424514110495879)
XLA Ops:
  0.0 184.2 %layer.1 = (bf16[512,1024]{1,0:T(8,128)(2,1)S(1)}, f32[8,512]{1,0:T(8,128)S(1)}) custom-call(bf16[512,1024]{1,0:T(8,128)(2,1)} %tokens_hbm.1, s32[4,512]{1,0:T(4,128)} %bitcast.4, f32[4,512]{1,0:T(4,128)} %bitcast.5, f32[1,1024]{1,0:T(1,128)} %bitcast.6, f32[1,1024]{1,0:T(1,128)} %bitcast.7, bf16[4,1024,512]{2,1,0:T(8,128)(2,1)} %gate_hbm.1, ...), custom_call_target="tpu_custom_call" | custom-call | tf_op jit(solution)/shard_map/layer/pallas_call | solution.py:781
  184.2 1.2 finish.1
